TPU v7x, 32 devices: a whole 2x2x4 slice. The times are simulated.
32 devices in a mesh: rep: 2 (over x), fs: 8 (over z, y), tp: 2 (over core).
Axes of the slice: x: 2, y: 2, z: 4, core: 2. Of those that a mesh axis runs over, the one named last changes fastest.
Arguments:
- tokens: bfloat16 [2048, 2048], P(('rep', 'fs')), may hold values from -6 to 6
- attention_norm_gain: float32 [2048], replicated, may hold values from 0.1 to 1.9
- query_weight: bfloat16 [2048, 1024], P('fs', 'tp'), may hold values from -0.125 to 0.125
- key_weight: bfloat16 [2048, 1024], P('fs', 'tp'), may hold values from -0.125 to 0.125
- value_weight: bfloat16 [2048, 2048], P('fs', 'tp'), may hold values from -0.125 to 0.125
- decay_weight: bfloat16 [2048, 1024], P('fs', 'tp'), may hold values from -0.125 to 0.125
- decay_gate_bias: float32 [1024], P('tp'), may hold values from -1.5 to 5.5
- decay_spike_extra: float32 [2048, 32], P(('rep', 'fs'), 'tp'), may hold values from -0.7 to 0
- head_output_gain: float32 [64], replicated, may hold values from 0.1 to 1.9
- output_weight: bfloat16 [2048, 2048], P('fs', 'tp'), may hold values from -0.125 to 0.125
- channel_norm_gain: float32 [2048], replicated, may hold values from 0.1 to 1.9
- gate_weight: bfloat16 [2048, 3072], P('fs', 'tp'), may hold values from -0.125 to 0.125
- up_weight: bfloat16 [2048, 3072], P('fs', 'tp'), may hold values from -0.125 to 0.125
- down_weight: bfloat16 [2048, 3072], P('fs', 'tp'), may hold values from -0.109375 to 0.109375
Outputs:
- layer_out: bfloat16 [2048, 2048], P(('rep', 'fs'))
All inputs are finite; a program needn't handle non-finite values.
Results may differ from a plain program's by a relative error of at most 0.018.
Values may be sent and summed in bfloat16 or wider, within the bound.
A program may use at most 128 MiB of HBM per device.

v0:
```python
import jax
import jax.numpy as jnp
from jax import lax
from jax.sharding import PartitionSpec as P

BLOCK = 64
GATE_NORM = 16.0
NORM_EPS = 1e-06
HIGHEST = lax.Precision.HIGHEST


def rms_scale(values, scales):
    floats = values.astype(jnp.float32)
    return floats * lax.rsqrt(jnp.mean(floats * floats, axis=-1, keepdims=True) + NORM_EPS) * scales


def one_way(queries, key_rows, value_rows, decay_logarithm):
    length, number_of_heads, key_width = queries.shape
    value_width = value_rows.shape[2]
    block_count = length // BLOCK

    def blocks(tensor):
        return tensor.reshape(block_count, BLOCK, number_of_heads, tensor.shape[2]).transpose(
            0, 2, 1, 3
        )

    lower_mask = jnp.tril(jnp.ones((BLOCK, BLOCK), bool))

    def advance(carried, pieces):
        query_part, key_part, value_part, decay_part = pieces
        running = jnp.cumsum(decay_part, axis=1)
        spread = jnp.where(
            lower_mask[None, :, :, None], running[:, :, None, :] - running[:, None, :, :], -jnp.inf
        )
        scores = jnp.einsum(
            "hid,hjd,hijd->hij", query_part, key_part, jnp.exp(spread), precision=HIGHEST
        )
        block_end = running[:, -1:, :]
        result = jnp.einsum("hij,hje->hie", scores, value_part, precision=HIGHEST)
        result = result + jnp.einsum(
            "hid,hde->hie", query_part * jnp.exp(running), carried, precision=HIGHEST
        )
        carried = jnp.exp(block_end)[:, 0, :, None] * carried + jnp.einsum(
            "hjd,hje->hde", key_part * jnp.exp(block_end - running), value_part, precision=HIGHEST
        )
        return (carried, result)

    zero_state = jnp.zeros((number_of_heads, key_width, value_width), jnp.float32)
    _, outputs = lax.scan(
        advance,
        zero_state,
        (blocks(queries), blocks(key_rows), blocks(value_rows), blocks(decay_logarithm)),
    )
    return outputs.transpose(0, 2, 1, 3).reshape(length, number_of_heads, value_width)


def both_ways(queries, key_rows, value_rows, decay_logarithm):
    forward = one_way(queries, key_rows, value_rows, decay_logarithm)
    backward = one_way(
        jnp.flip(queries, 0),
        jnp.flip(key_rows, 0),
        jnp.flip(value_rows, 0),
        jnp.flip(decay_logarithm, 0),
    )
    return forward + jnp.flip(backward, 0)


def rounded(floats):
    return lax.optimization_barrier(floats.astype(jnp.bfloat16)).astype(jnp.float32)


def shards(
    tokens,
    attention_norm_gain,
    query_weight,
    key_weight,
    value_weight,
    decay_weight,
    decay_gate_bias,
    decay_spike_extra,
    head_output_gain,
    output_weight,
    channel_norm_gain,
    gate_weight,
    up_weight,
    down_weight,
):
    full_query, full_key, full_value, full_decay, full_output = (
        lax.all_gather(query_weight, "fs", axis=0, tiled=True),
        lax.all_gather(key_weight, "fs", axis=0, tiled=True),
        lax.all_gather(value_weight, "fs", axis=0, tiled=True),
        lax.all_gather(decay_weight, "fs", axis=0, tiled=True),
        lax.all_gather(output_weight, "fs", axis=0, tiled=True),
    )
    normed = rms_scale(tokens, attention_norm_gain).astype(jnp.bfloat16)
    narrow = full_query.shape[1]
    wide_cols = full_value.shape[1]
    length = normed.shape[0]
    number_of_heads = decay_spike_extra.shape[1]
    key_width = narrow // number_of_heads
    value_width = wide_cols // number_of_heads
    query_proj = jnp.dot(normed, full_query, preferred_element_type=jnp.float32)
    key_proj = jnp.dot(normed, full_key, preferred_element_type=jnp.float32)
    value_proj = jnp.dot(normed, full_value, preferred_element_type=jnp.float32)
    gate_pre = jnp.dot(normed, full_decay, preferred_element_type=jnp.float32)
    queries = (rounded(query_proj) * key_width ** (-0.5)).reshape(
        length, number_of_heads, key_width
    )
    key_rows = rounded(key_proj).reshape(length, number_of_heads, key_width)
    value_rows = rounded(value_proj).reshape(length, number_of_heads, value_width)
    decay_logarithm = (
        jax.nn.log_sigmoid(gate_pre + decay_gate_bias).reshape(length, number_of_heads, key_width)
        / GATE_NORM
    )
    decay_logarithm = decay_logarithm + decay_spike_extra[:, :, None]
    mixed_heads = both_ways(queries, key_rows, value_rows, decay_logarithm)
    attended = (
        rms_scale(mixed_heads, head_output_gain).reshape(length, wide_cols).astype(jnp.bfloat16)
    )
    full_gate, full_up, full_down = (
        lax.all_gather(gate_weight, "fs", axis=0, tiled=True),
        lax.all_gather(up_weight, "fs", axis=0, tiled=True),
        lax.all_gather(down_weight, "fs", axis=0, tiled=True),
    )
    mixer_term = lax.dot_general(
        attended, full_output, (((1,), (1,)), ((), ())), preferred_element_type=jnp.float32
    )
    mixed_sum = lax.psum(mixer_term.astype(jnp.bfloat16), "tp").astype(jnp.float32)
    residual = (tokens.astype(jnp.float32) + mixed_sum).astype(jnp.bfloat16)
    normed_two = rms_scale(residual, channel_norm_gain).astype(jnp.bfloat16)
    gate_part = jnp.dot(normed_two, full_gate, preferred_element_type=jnp.float32)
    up_part = jnp.dot(normed_two, full_up, preferred_element_type=jnp.float32)
    hidden = (jax.nn.silu(gate_part) * up_part).astype(jnp.bfloat16)
    channel_term = lax.dot_general(
        hidden, full_down, (((1,), (1,)), ((), ())), preferred_element_type=jnp.float32
    )
    channel_sum = lax.psum(channel_term.astype(jnp.bfloat16), "tp").astype(jnp.float32)
    return (residual.astype(jnp.float32) + channel_sum).astype(jnp.bfloat16)


def solution(mesh):
    in_specs = (
        P(("rep", "fs"), None),
        P(),
        P("fs", "tp"),
        P("fs", "tp"),
        P("fs", "tp"),
        P("fs", "tp"),
        P("tp"),
        P(("rep", "fs"), "tp"),
        P(),
        P("fs", "tp"),
        P(),
        P("fs", "tp"),
        P("fs", "tp"),
        P("fs", "tp"),
    )
    out_specs = P(("rep", "fs"), None)
    return jax.shard_map(shards, mesh=mesh, in_specs=in_specs, out_specs=out_specs, check_vma=False)
```

profile of v0, /device:TPU:0, one launch (start us, length us, event | category | flops | bytes accessed | tf_op | source)
XLA Modules:
  0.0 797.3 jit_solution(2030128879946733997)
XLA Ops:
  12.0 49.3 %all-gather.9.cloned.1.call-done = bf16[2048,512]{1,0:T(8,128)(2,1)} async-done(((bf16[256,512]{1,0:T(8,128)(2,1)}), bf16[2048,512]{1,0:T(8,128)(2,1)}) %all-gather.9.cloned.1.call-update) | async-done | bytes 2097168 | tf_op jit(solution)/shard_map/all_gather | solution.py:92
  61.3 2.4 fusion.48
  65.7 45.4 %all-gather.15.cloned.1.call-done = bf16[2048,512]{1,0:T(8,128)(2,1)} async-done(((bf16[256,512]{1,0:T(8,128)(2,1)}), bf16[2048,512]{1,0:T(8,128)(2,1)}) %all-gather.15.cloned.1.call-update) | async-done | bytes 2097168 | tf_op jit(solution)/shard_map/all_gather | solution.py:89
  115.1 45.8 %all-gather.11.cloned.1.call-done = bf16[2048,512]{1,0:T(8,128)(2,1)} async-done(((bf16[256,512]{1,0:T(8,128)(2,1)}), bf16[2048,512]{1,0:T(8,128)(2,1)}) %all-gather.11.cloned.1.call-update) | async-done | bytes 2097168 | tf_op jit(solution)/shard_map/all_gather | solution.py:90
  166.7 67.5 %all-gather.13.cloned.1.call-done = bf16[2048,1024]{1,0:T(8,128)(2,1)} async-done(((bf16[256,1024]{1,0:T(8,128)(2,1)}), bf16[2048,1024]{1,0:T(8,128)(2,1)}) %all-gather.13.cloned.1.call-update) | async-done | bytes 4194320 | tf_op jit(solution)/shard_map/all_gather | solution.py:91
  234.2 2.9 convolution_convert_fusion.2
  241.6 90.0 %while.27 = (s32[]{:T(128)}, f32[16,32,64]{2,1,0:T(8,128)}, f32[2,16,64,64]{3,2,1,0:T(8,128)}, f32[2,16,64,32]{3,1,2,0:T(8,128)}, f32[2,16,64,32]{3,1,2,0:T(8,12...) while((s32[]{:T(128)}, f32[16,32,64]{2,1,0:T(8,128)}, ...), condition=%wide.region_6.7_spmd.clone, body=%wide.region_4.6_spmd.clone.sunk | while | flops 113446912 | bytes 41307280 | solution.py:49
  243.1 8.4 %select_exponential_fusion.5 = f32[16,64,64,32]{2,3,1,0:T(8,128)} fusion(f32[16,64,32]{1,2,0:T(8,128)S(1)} %copy.175, f32[16,64,32]{2,1,0:T(8,128)S(1)} %copy.176, pred[64,64]{1,0:T(8,128)(4,1)S(1)} %iota_compare_fusion.5), kind=kLoop, calls=%fused_computation.34.clone.1 | loop fusion | flops 4194304 | bytes 8654848 | tf_op jit(solution)/shard_map/while/body/eval_jaxpr/exp | solution.py:36
  251.5 18.5 %copy.177 = f32[16,64,64,32]{1,2,3,0:T(8,128)} copy(f32[16,64,64,32]{2,3,1,0:T(8,128)} %select_exponential_fusion.5) | data formatting | bytes 16777216 | tf_op jit(solution)/shard_map/while
  271.6 7.7 fusion.114
  287.2 8.4 %select_exponential_fusion.5 = f32[16,64,64,32]{2,3,1,0:T(8,128)} fusion(f32[16,64,32]{1,2,0:T(8,128)S(1)} %copy.175, f32[16,64,32]{2,1,0:T(8,128)S(1)} %copy.176, pred[64,64]{1,0:T(8,128)(4,1)S(1)} %iota_compare_fusion.5), kind=kLoop, calls=%fused_computation.34.clone.1 | loop fusion | flops 4194304 | bytes 8654848 | tf_op jit(solution)/shard_map/while/body/eval_jaxpr/exp | solution.py:36
  295.6 18.4 %copy.177 = f32[16,64,64,32]{1,2,3,0:T(8,128)} copy(f32[16,64,64,32]{2,3,1,0:T(8,128)} %select_exponential_fusion.5) | data formatting | bytes 16777216 | tf_op jit(solution)/shard_map/while
  315.6 7.7 fusion.114
  328.8 2.7 convolution_add_fusion.8
  334.7 2.5 copy.149
  338.4 98.9 %while.26 = (s32[]{:T(128)}, f32[16,32,64]{2,1,0:T(8,128)S(1)}, f32[2,16,64,64]{3,2,1,0:T(8,128)}, f32[2,16,64,32]{2,0,3,1:T(2,128)}, f32[2,16,64,32]{2,0,3,1:T(...) while((s32[]{:T(128)}, f32[16,32,64]{2,1,0:T(8,128)S(1)}, ...), condition=%wide.region_3.4_spmd.clone, body=%wide.region_1.3_spmd.clone.sunk | while | flops 113446912 | bytes 47736008 | solution.py:49
  340.0 6.3 fusion.101
  350.0 8.4 %select_exponential_fusion.4 = f32[16,64,64,32]{2,3,1,0:T(8,128)} fusion(f32[16,64,32]{1,2,0:T(8,128)S(1)} %copy.170, f32[16,64,32]{2,1,0:T(8,128)S(1)} %copy.171, pred[64,64]{1,0:T(8,128)(4,1)S(1)} %iota_compare_fusion.4), kind=kLoop, calls=%fused_computation.4.clone.1 | loop fusion | flops 4194304 | bytes 8654848 | tf_op jit(solution)/shard_map/while/body/eval_jaxpr/exp | solution.py:36
  358.4 18.4 %copy.172 = f32[16,64,64,32]{1,2,3,0:T(8,128)} copy(f32[16,64,64,32]{2,3,1,0:T(8,128)} %select_exponential_fusion.4) | data formatting | bytes 16777216 | tf_op jit(solution)/shard_map/while
  376.8 7.8 fusion.103
  389.4 6.3 fusion.101
  399.5 8.4 %select_exponential_fusion.4 = f32[16,64,64,32]{2,3,1,0:T(8,128)} fusion(f32[16,64,32]{1,2,0:T(8,128)S(1)} %copy.170, f32[16,64,32]{2,1,0:T(8,128)S(1)} %copy.171, pred[64,64]{1,0:T(8,128)(4,1)S(1)} %iota_compare_fusion.4), kind=kLoop, calls=%fused_computation.4.clone.1 | loop fusion | flops 4194304 | bytes 8654848 | tf_op jit(solution)/shard_map/while/body/eval_jaxpr/exp | solution.py:36
  407.9 18.4 %copy.172 = f32[16,64,64,32]{1,2,3,0:T(8,128)} copy(f32[16,64,64,32]{2,3,1,0:T(8,128)} %select_exponential_fusion.4) | data formatting | bytes 16777216 | tf_op jit(solution)/shard_map/while
  426.3 7.8 fusion.103
  440.8 4.5 convolution_convert_fusion.1
  447.9 14.8 %all-reduce.3.cloned.1.call-done = bf16[128,2048]{1,0:T(8,128)(2,1)} async-done(((bf16[128,2048]{1,0:T(8,128)(2,1)}), bf16[128,2048]{1,0:T(8,128)(2,1)}) %all-reduce.3.cloned.1.call-update) | async-done | bytes 524304 | tf_op jit(solution)/shard_map/psum | solution.py:128
  464.0 100.8 %all-gather.19.cloned.1.call-done = bf16[2048,1536]{1,0:T(8,128)(2,1)} async-done(((bf16[256,1536]{1,0:T(8,128)(2,1)}), bf16[2048,1536]{1,0:T(8,128)(2,1)}) %all-gather.19.cloned.1.call-update) | async-done | bytes 6291472 | tf_op jit(solution)/shard_map/all_gather | solution.py:121
  564.8 3.8 fusion.51
  568.6 95.3 %all-gather.21.cloned.1.call-done = bf16[2048,1536]{1,0:T(8,128)(2,1)} async-done(((bf16[256,1536]{1,0:T(8,128)(2,1)}), bf16[2048,1536]{1,0:T(8,128)(2,1)}) %all-gather.21.cloned.1.call-update) | async-done | bytes 6291472 | tf_op jit(solution)/shard_map/all_gather | solution.py:122
  663.9 99.1 %all-gather.23.cloned.1.call-done = bf16[2048,1536]{1,0:T(8,128)(2,1)} async-done(((bf16[256,1536]{1,0:T(8,128)(2,1)}), bf16[2048,1536]{1,0:T(8,128)(2,1)}) %all-gather.23.cloned.1.call-update) | async-done | bytes 6291472 | tf_op jit(solution)/shard_map/all_gather | solution.py:123
  763.0 8.6 %convolution_convert_fusion = bf16[128,2048]{1,0:T(8,128)(2,1)} fusion(bf16[2048,1536]{1,0:T(8,128)(2,1)} %all-gather.23.cloned.1.call-done, bf16[2048,1536]{1,0:T(8,128)(2,1)} %all-gather.21.cloned.1.call-done, f32[128,1536]{1,0:T(8,128)S(1)} %fusion.51, bf16[128,2048]{1,0:T(8,128)(2,1)S(1)} %get-tuple-element.214, f32[2048]{0:T(1024)S(1)} %copy-done.8, ...), kind=kOutput, calls=%fused_computation.60 | convolution fusion | flops 1613103104 | bytes 14426624 | tf_op jit(solution)/shard_map/dot_general | solution.py:134
  771.5 16.9 %all-reduce.5.cloned.1.call-done = bf16[128,2048]{1,0:T(8,128)(2,1)} async-done(((bf16[128,2048]{1,0:T(8,128)(2,1)}), bf16[128,2048]{1,0:T(8,128)(2,1)}) %all-reduce.5.cloned.1.call-update) | async-done | bytes 524304 | tf_op jit(solution)/shard_map/psum | solution.py:137
  (139 shorter events, 69.9 us)
Async XLA Ops:
  6.5 104.5 %copy-start.2 = (bf16[128,2048]{1,0:T(8,128)(2,1)S(1)}, bf16[128,2048]{1,0:T(8,128)(2,1)}, u32[]{:S(2)}) copy-start(bf16[128,2048]{1,0:T(8,128)(2,1)} %param.18) | copy-start | bytes 1572868
  6.5 57.7 %copy-start.6 = (f32[128,16]{0,1:T(8,128)S(1)}, f32[128,16]{0,1:T(8,128)}, u32[]{:S(2)}) copy-start(f32[128,16]{0,1:T(8,128)} %param.25) | copy-start | bytes 24580
  6.5 104.5 %copy-start.7 = (f32[2048]{0:T(1024)S(1)}, f32[2048]{0:T(1024)}, u32[]{:S(2)}) copy-start(f32[2048]{0:T(1024)} %param.19) | copy-start | bytes 24580
  6.5 54.8 %all-gather.9.cloned.1.call-start = ((), (), s32[]{:S(2)}) async-start(), calls=%async_computation | async-start | bytes 2359296 | tf_op jit(solution)/shard_map/all_gather | solution.py:92
  7.3 103.8 %all-gather.15.cloned.1.call-start = ((), (), s32[]{:S(2)}) async-start(), calls=%async_computation.3 | async-start | bytes 2359296 | tf_op jit(solution)/shard_map/all_gather | solution.py:89
  8.0 152.9 %all-gather.11.cloned.1.call-start = ((), (), s32[]{:S(2)}) async-start(), calls=%async_computation.1 | async-start | bytes 2359296 | tf_op jit(solution)/shard_map/all_gather | solution.py:90
  8.7 225.5 %all-gather.13.cloned.1.call-start = ((), (), s32[]{:S(2)}) async-start(), calls=%async_computation.2 | async-start | bytes 4718592 | tf_op jit(solution)/shard_map/all_gather | solution.py:91
  9.3 431.5 %all-gather.17.cloned.1.call-start = ((), (), s32[]{:S(2)}) async-start(), calls=%async_computation.4 | async-start | bytes 4718592 | tf_op jit(solution)/shard_map/all_gather | solution.py:93
  9.9 452.7 %all-reduce.3.cloned.1.call-start = ((), (), s32[]{:S(2)}) async-start(), calls=%async_computation.5 | async-start | bytes 1048576 | tf_op jit(solution)/shard_map/psum | solution.py:128
  271.6 7.7 copy-start
  315.6 7.7 copy-start
  338.4 102.2 %copy-start.9 = (f32[64]{0:T(128)S(1)}, f32[64]{0:T(128)}, u32[]{:S(2)}) copy-start(f32[64]{0:T(128)} %param.26) | copy-start | bytes 772
  376.8 7.8 copy-start.1
  376.8 7.9 copy-start.4
  385.7 1.0 copy-start.5
  426.3 7.8 copy-start.1
  426.3 7.9 copy-start.4
  435.2 1.0 copy-start.5
  438.9 23.8 %copy-start.3 = (bf16[128,2048]{1,0:T(8,128)(2,1)S(1)}, bf16[128,2048]{1,0:T(8,128)(2,1)}, u32[]{:S(2)}) copy-start(bf16[128,2048]{1,0:T(8,128)(2,1)} %param.18) | copy-start | bytes 1572868
  439.5 125.3 %copy-start.8 = (f32[2048]{0:T(1024)S(1)}, f32[2048]{0:T(1024)}, u32[]{:S(2)}) copy-start(f32[2048]{0:T(1024)} %param.28) | copy-start | bytes 24580
  445.3 119.5 %all-gather.19.cloned.1.call-start = ((), (), s32[]{:S(2)}) async-start(), calls=%async_computation.6 | async-start | bytes 7077888 | tf_op jit(solution)/shard_map/all_gather | solution.py:121
  446.1 217.8 %all-gather.21.cloned.1.call-start = ((), (), s32[]{:S(2)}) async-start(), calls=%async_computation.7 | async-start | bytes 7077888 | tf_op jit(solution)/shard_map/all_gather | solution.py:122
  446.8 316.1 %all-gather.23.cloned.1.call-start = ((), (), s32[]{:S(2)}) async-start(), calls=%async_computation.8 | async-start | bytes 7077888 | tf_op jit(solution)/shard_map/all_gather | solution.py:123
  447.5 340.9 %all-reduce.5.cloned.1.call-start = ((), (), s32[]{:S(2)}) async-start(), calls=%async_computation.9 | async-start | bytes 1048576 | tf_op jit(solution)/shard_map/psum | solution.py:137
Sparse Core Ops, SparseCore 0:
  9.5 51.7 all-gather.8
  63.4 47.6 all-gather.14
  113.2 47.6 all-gather.10
  162.8 71.3 all-gather.12
  236.2 71.3 all-gather.16
  445.4 17.1 all-reduce.2
  464.8 99.8 all-gather.18
  566.9 96.8 all-gather.20
  666.0 96.8 all-gather.22
  771.7 16.7 all-reduce.4
where the time goes:
time: 799 us; the launch traced here: 797 us
  waiting for transfers between devices  540 us (68%)
  local copies, waits for them, and re-layouts  113 us (14%)
  other arithmetic  87 us (11%)
  matrix products  42.7 us (5%)
  between operations  13.8 us (2%)
    all_gather x1, waiting for transfers between devices, shards(): lax.all_gather(gate_weight, 'fs', axis=0, tiled=True)  101 us
    all_gather x1, waiting for transfers between devices, shards(): lax.all_gather(down_weight, 'fs', axis=0, tiled=True)  99.1 us
    all_gather x1, waiting for transfers between devices, shards(): lax.all_gather(up_weight, 'fs', axis=0, tiled=True)  95.3 us
    while x20, local copies, waits for them, and re-layouts  75.6 us
    all_gather x1, waiting for transfers between devices, shards(): lax.all_gather(value_weight, 'fs', axis=0, tiled=True)  67.5 us
    all_gather x1, waiting for transfers between devices, shards(): lax.all_gather(decay_weight, 'fs', axis=0, tiled=True)  49.3 us
    all_gather x1, waiting for transfers between devices, shards(): lax.all_gather(key_weight, 'fs', axis=0, tiled=True)  45.8 us
    all_gather x1, waiting for transfers between devices, shards(): lax.all_gather(query_weight, 'fs', axis=0, tiled=True)  45.4 us
  transfers between devices with their start and end apart: 10, of which 9 were waited for; matrix products, arithmetic and copies ran while one was open for 28% of the time, Pallas kernels for 0%

commit v1 on v0

--- a/solution.py
+++ b/solution.py
@@ -2,6 +2,7 @@
 import jax.numpy as jnp
 from jax import lax
 from jax.sharding import PartitionSpec as P
+from jax.lax import axis_index, axis_size, ppermute
 
 BLOCK = 64
 GATE_NORM = 16.0
@@ -117,9 +118,35 @@
     attended = (
         rms_scale(mixed_heads, head_output_gain).reshape(length, wide_cols).astype(jnp.bfloat16)
     )
+
+    def _choose_tracks(own_rows):
+        extra = axis_size("fs")
+        base_arr = axis_index("fs")
+        u1, all_values, local_next = (extra, base_arr, own_rows.shape[0])
+        carry_out = jnp.zeros(
+            [i0 * u1 if kk == 0 else i0 for kk, i0 in enumerate(own_rows.shape)], own_rows.dtype
+        )
+        all_rows = lax.dynamic_update_slice_in_dim(
+            carry_out, own_rows, all_values * local_next, axis=0
+        )
+        far_arr = d_next = own_rows
+        for tick in range(1, u1 // 2 + 1):
+            z1 = list(map(lambda kk: (kk, (kk + 1) % u1), range(u1)))
+            far_arr = ppermute(far_arr, "fs", z1)
+            all_rows = lax.dynamic_update_slice_in_dim(
+                all_rows, far_arr, (all_values - tick) % u1 * local_next, axis=0
+            )
+            if 2 * tick < u1:
+                built = list(map(lambda kk: (kk, (kk - 1) % u1), range(u1)))
+                d_next = ppermute(d_next, "fs", built)
+                all_rows = lax.dynamic_update_slice_in_dim(
+                    all_rows, d_next, (all_values + tick) % u1 * local_next, axis=0
+                )
+        return all_rows
+
     full_gate, full_up, full_down = (
         lax.all_gather(gate_weight, "fs", axis=0, tiled=True),
-        lax.all_gather(up_weight, "fs", axis=0, tiled=True),
+        _choose_tracks(up_weight),
         lax.all_gather(down_weight, "fs", axis=0, tiled=True),
     )
     mixer_term = lax.dot_general(

time: 799 us -> 771 us (0.965)
  waiting for transfers between devices: 540 us -> 478 us
  local copies, waits for them, and re-layouts: 113 us -> 129 us
  starting transfers between devices: 0.61 us -> 15.1 us
    ppermute x0 -> x7, waiting for transfers between devices: none -> 132 us  [the longest x4 124 us: _choose_tracks(): far_arr = ppermute(far_arr, 'fs', z1)]
    all_gather x1 -> x0, waiting for transfers between devices: 95.3 us -> none  [shards(): lax.all_gather(up_weight, 'fs', axis=0, tiled=True)]
    all_gather x1, waiting for transfers between devices: 101 us -> 20.4 us  [shards(): lax.all_gather(gate_weight, 'fs', axis=0, tiled=True)]
    ppermute x0 -> x7, starting transfers between devices: none -> 14.8 us  [the longest x4 7.67 us: _choose_tracks(): far_arr = ppermute(far_arr, 'fs', z1)]
    psum x1, waiting for transfers between devices: 14.8 us -> 0.01 us  [shards(): lax.psum(mixer_term.astype(jnp.bfloat16), 'tp').astype(jnp.float32)]
    dynamic_update_slice x0 -> x8, local copies, waits for them, and re-layouts: none -> 11 us  [the longest x3 5.08 us: _choose_tracks(): lax.dynamic_update_slice_in_dim(all_rows, d_next, (all_values + tick) % u...]
    while x20 -> x32, local copies, waits for them, and re-layouts: 75.6 us -> 77.5 us
  transfers between devices with their start and end apart: 10 -> 16, of which waited for: 9 -> 13; matrix products, arithmetic and copies ran while one was open for 28% -> 32% of each run, Pallas kernels for 0% -> 0%
where the time goes in v1:
time: 771 us; the launch traced here: 769 us
  waiting for transfers between devices  478 us (62%)
  local copies, waits for them, and re-layouts  129 us (17%)
  other arithmetic  90.1 us (12%)
  matrix products  43.2 us (6%)
  starting transfers between devices  15.1 us (2%)
  between operations  13.5 us (2%)
    ppermute x4, waiting for transfers between devices, _choose_tracks(): far_arr = ppermute(far_arr, 'fs', z1)  124 us
    all_gather x1, waiting for transfers between devices, shards(): lax.all_gather(down_weight, 'fs', axis=0, tiled=True)  95.9 us
    while x32, local copies, waits for them, and re-layouts  77.5 us
    all_gather x1, waiting for transfers between devices, shards(): lax.all_gather(value_weight, 'fs', axis=0, tiled=True)  64.4 us
    all_gather x1, waiting for transfers between devices, shards(): lax.all_gather(decay_weight, 'fs', axis=0, tiled=True)  49.3 us
    all_gather x1, waiting for transfers between devices, shards(): lax.all_gather(query_weight, 'fs', axis=0, tiled=True)  47.3 us
    all_gather x1, waiting for transfers between devices, shards(): lax.all_gather(key_weight, 'fs', axis=0, tiled=True)  46.9 us
    exp x4, other arithmetic, advance(): jnp.exp(spread)  34.2 us
  transfers between devices with their start and end apart: 16, of which 13 were waited for; matrix products, arithmetic and copies ran while one was open for 32% of the time, Pallas kernels for 0%

profile of v1, /device:TPU:0, one launch (start us, length us, event | category | flops | bytes accessed | tf_op | source)
XLA Modules:
  0.0 768.8 jit_solution(8184539226253125712)
XLA Ops:
  12.0 49.3 %all-gather.8.cloned.1.call-done = bf16[2048,512]{1,0:T(8,128)(2,1)} async-done(((bf16[256,512]{1,0:T(8,128)(2,1)}), bf16[2048,512]{1,0:T(8,128)(2,1)}) %all-gather.8.cloned.1.call-update) | async-done | bytes 2097168 | tf_op jit(solution)/shard_map/all_gather | solution.py:93
  64.2 46.9 %all-gather.10.cloned.1.call-done = bf16[2048,512]{1,0:T(8,128)(2,1)} async-done(((bf16[256,512]{1,0:T(8,128)(2,1)}), bf16[2048,512]{1,0:T(8,128)(2,1)}) %all-gather.10.cloned.1.call-update) | async-done | bytes 2097168 | tf_op jit(solution)/shard_map/all_gather | solution.py:91
  113.6 47.3 %all-gather.14.cloned.1.call-done = bf16[2048,512]{1,0:T(8,128)(2,1)} async-done(((bf16[256,512]{1,0:T(8,128)(2,1)}), bf16[2048,512]{1,0:T(8,128)(2,1)}) %all-gather.14.cloned.1.call-update) | async-done | bytes 2097168 | tf_op jit(solution)/shard_map/all_gather | solution.py:90
  169.8 64.4 %all-gather.12.cloned.1.call-done = bf16[2048,1024]{1,0:T(8,128)(2,1)} async-done(((bf16[256,1024]{1,0:T(8,128)(2,1)}), bf16[2048,1024]{1,0:T(8,128)(2,1)}) %all-gather.12.cloned.1.call-update) | async-done | bytes 4194320 | tf_op jit(solution)/shard_map/all_gather | solution.py:92
  240.8 101.7 %while.26 = (s32[]{:T(128)}, f32[16,32,64]{2,1,0:T(8,128)S(1)}, f32[2,16,64,64]{3,2,1,0:T(8,128)}, f32[2,16,64,32]{2,0,3,1:T(2,128)}, f32[2,16,64,32]{2,0,3,1:T(...) while((s32[]{:T(128)}, f32[16,32,64]{2,1,0:T(8,128)S(1)}, ...), condition=%wide.region_3.4_spmd.clone, body=%wide.region_1.3_spmd.clone.sunk | while | flops 113446912 | bytes 49302792 | solution.py:50
  244.6 6.3 fusion.101
  254.7 8.6 %select_exponential_fusion.4 = f32[16,64,64,32]{2,3,1,0:T(8,128)} fusion(f32[16,64,32]{1,2,0:T(8,128)S(1)} %copy.170, f32[16,64,32]{2,1,0:T(8,128)S(1)} %copy.171, pred[64,64]{1,0:T(8,128)(4,1)S(1)} %iota_compare_fusion.4), kind=kLoop, calls=%fused_computation.4.clone.1 | loop fusion | flops 4194304 | bytes 8654848 | tf_op jit(solution)/shard_map/while/body/eval_jaxpr/exp | solution.py:37
  263.3 18.4 %copy.172 = f32[16,64,64,32]{1,2,3,0:T(8,128)} copy(f32[16,64,64,32]{2,3,1,0:T(8,128)} %select_exponential_fusion.4) | data formatting | bytes 16777216 | tf_op jit(solution)/shard_map/while
  281.7 8.0 %fusion.103 = f32[16,64,64]{1,2,0:T(8,128)S(1)} fusion(f32[16,64,64,32]{1,2,3,0:T(8,128)} %copy.172, f32[16,32,64]{2,1,0:T(8,128)S(1)} %bitcast.159, f32[16,32,64]{2,1,0:T(8,128)S(1)} %bitcast.160), kind=kLoop, calls=%fused_computation.3.clone.1 | loop fusion | flops 6225920 | bytes 8912896 | tf_op jit(solution)/shard_map/while/body/eval_jaxpr/hid,hjd,hijd->hij/dot_general | solution.py:36
  295.5 6.3 fusion.101
  305.6 8.6 %select_exponential_fusion.4 = f32[16,64,64,32]{2,3,1,0:T(8,128)} fusion(f32[16,64,32]{1,2,0:T(8,128)S(1)} %copy.170, f32[16,64,32]{2,1,0:T(8,128)S(1)} %copy.171, pred[64,64]{1,0:T(8,128)(4,1)S(1)} %iota_compare_fusion.4), kind=kLoop, calls=%fused_computation.4.clone.1 | loop fusion | flops 4194304 | bytes 8654848 | tf_op jit(solution)/shard_map/while/body/eval_jaxpr/exp | solution.py:37
  314.2 18.4 %copy.172 = f32[16,64,64,32]{1,2,3,0:T(8,128)} copy(f32[16,64,64,32]{2,3,1,0:T(8,128)} %select_exponential_fusion.4) | data formatting | bytes 16777216 | tf_op jit(solution)/shard_map/while
  332.5 8.0 %fusion.103 = f32[16,64,64]{1,2,0:T(8,128)S(1)} fusion(f32[16,64,64,32]{1,2,3,0:T(8,128)} %copy.172, f32[16,32,64]{2,1,0:T(8,128)S(1)} %bitcast.159, f32[16,32,64]{2,1,0:T(8,128)S(1)} %bitcast.160), kind=kLoop, calls=%fused_computation.3.clone.1 | loop fusion | flops 6225920 | bytes 8912896 | tf_op jit(solution)/shard_map/while/body/eval_jaxpr/hid,hjd,hijd->hij/dot_general | solution.py:36
  349.6 92.6 %while.27 = (s32[]{:T(128)}, f32[16,32,64]{2,1,0:T(8,128)}, f32[2,16,64,64]{3,2,1,0:T(8,128)}, f32[2,16,64,32]{3,1,2,0:T(8,128)}, f32[2,16,64,32]{3,1,2,0:T(8,12...) while((s32[]{:T(128)}, f32[16,32,64]{2,1,0:T(8,128)}, ...), condition=%wide.region_6.7_spmd.clone, body=%wide.region_4.6_spmd.clone.sunk | while | flops 113446912 | bytes 45238460 | solution.py:50
  356.7 8.6 %select_exponential_fusion.5 = f32[16,64,64,32]{2,3,1,0:T(8,128)} fusion(f32[16,64,32]{1,2,0:T(8,128)S(1)} %copy.175, f32[16,64,32]{2,1,0:T(8,128)S(1)} %copy.176, pred[64,64]{1,0:T(8,128)(4,1)S(1)} %iota_compare_fusion.5), kind=kLoop, calls=%fused_computation.34.clone.1 | loop fusion | flops 4194304 | bytes 8654848 | tf_op jit(solution)/shard_map/while/body/eval_jaxpr/exp | solution.py:37
  365.3 18.4 %copy.177 = f32[16,64,64,32]{1,2,3,0:T(8,128)} copy(f32[16,64,64,32]{2,3,1,0:T(8,128)} %select_exponential_fusion.5) | data formatting | bytes 16777216 | tf_op jit(solution)/shard_map/while
  385.3 7.7 fusion.114
  404.0 8.6 %select_exponential_fusion.5 = f32[16,64,64,32]{2,3,1,0:T(8,128)} fusion(f32[16,64,32]{1,2,0:T(8,128)S(1)} %copy.175, f32[16,64,32]{2,1,0:T(8,128)S(1)} %copy.176, pred[64,64]{1,0:T(8,128)(4,1)S(1)} %iota_compare_fusion.5), kind=kLoop, calls=%fused_computation.34.clone.1 | loop fusion | flops 4194304 | bytes 8654848 | tf_op jit(solution)/shard_map/while/body/eval_jaxpr/exp | solution.py:37
  412.6 18.4 %copy.177 = f32[16,64,64,32]{1,2,3,0:T(8,128)} copy(f32[16,64,64,32]{2,3,1,0:T(8,128)} %select_exponential_fusion.5) | data formatting | bytes 16777216 | tf_op jit(solution)/shard_map/while
  432.6 7.7 fusion.114
  446.0 4.5 convolution_convert_fusion.1
  452.7 4.1 collective-permute-start.1
  456.9 37.0 %collective-permute-done = bf16[256,1536]{1,0:T(8,128)(2,1)S(1)} collective-permute-done((bf16[256,1536]{1,0:T(8,128)(2,1)S(1)}, bf16[256,1536]{1,0:T(8,128)(2,1)S(1)}, u32[]{:S(2)}, u32[]{:S(2)}) %collective-permute-start) | collective-permute-done | bytes 786464 | tf_op jit(solution)/shard_map/ppermute | solution.py:135
  498.5 29.0 %collective-permute-done.2 = bf16[256,1536]{1,0:T(8,128)(2,1)} collective-permute-done((bf16[256,1536]{1,0:T(8,128)(2,1)S(1)}, bf16[256,1536]{1,0:T(8,128)(2,1)}, u32[]{:S(2)}, u32[]{:S(2)}) %collective-permute-start.2) | collective-permute-done | bytes 786464 | tf_op jit(solution)/shard_map/ppermute | solution.py:135
  539.3 41.6 %collective-permute-done.4 = bf16[256,1536]{1,0:T(8,128)(2,1)S(1)} collective-permute-done((bf16[256,1536]{1,0:T(8,128)(2,1)}, bf16[256,1536]{1,0:T(8,128)(2,1)S(1)}, u32[]{:S(2)}, u32[]{:S(2)}) %collective-permute-start.4) | collective-permute-done | bytes 786464 | tf_op jit(solution)/shard_map/ppermute | solution.py:135
  588.3 6.3 collective-permute-done.5
  595.6 16.8 %collective-permute-done.6 = bf16[256,1536]{1,0:T(8,128)(2,1)S(1)} collective-permute-done((bf16[256,1536]{1,0:T(8,128)(2,1)S(1)}, bf16[256,1536]{1,0:T(8,128)(2,1)S(1)}, u32[]{:S(2)}, u32[]{:S(2)}) %collective-permute-start.6) | collective-permute-done | bytes 786464 | tf_op jit(solution)/shard_map/ppermute | solution.py:135
  614.6 20.4 %all-gather.18.cloned.1.call-done = bf16[2048,1536]{1,0:T(8,128)(2,1)} async-done(((bf16[256,1536]{1,0:T(8,128)(2,1)}), bf16[2048,1536]{1,0:T(8,128)(2,1)}) %all-gather.18.cloned.1.call-update) | async-done | bytes 6291472 | tf_op jit(solution)/shard_map/all_gather | solution.py:148
  635.0 3.8 fusion.51
  638.9 95.9 %all-gather.20.cloned.1.call-done = bf16[2048,1536]{1,0:T(8,128)(2,1)} async-done(((bf16[256,1536]{1,0:T(8,128)(2,1)}), bf16[2048,1536]{1,0:T(8,128)(2,1)}) %all-gather.20.cloned.1.call-update) | async-done | bytes 6291472 | tf_op jit(solution)/shard_map/all_gather | solution.py:150
  734.7 8.6 %convolution_convert_fusion = bf16[128,2048]{1,0:T(8,128)(2,1)} fusion(bf16[2048,1536]{1,0:T(8,128)(2,1)} %all-gather.20.cloned.1.call-done, bf16[2048,1536]{1,0:T(8,128)(2,1)} %constant_dynamic-update-slice_fusion, f32[128,1536]{1,0:T(8,128)S(1)} %fusion.51, bf16[128,2048]{1,0:T(8,128)(2,1)S(1)} %get-tuple-element.214, f32[2048]{0:T(1024)S(1)} %copy-done.15, ...), kind=kOutput, calls=%fused_computation.60 | convolution fusion | flops 1613103104 | bytes 14426624 | tf_op jit(solution)/shard_map/dot_general | solution.py:161
  743.3 17.0 %all-reduce.5.cloned.1.call-done = bf16[128,2048]{1,0:T(8,128)(2,1)} async-done(((bf16[128,2048]{1,0:T(8,128)(2,1)}), bf16[128,2048]{1,0:T(8,128)(2,1)}) %all-reduce.5.cloned.1.call-update) | async-done | bytes 524304 | tf_op jit(solution)/shard_map/psum | solution.py:164
  (179 shorter events, 110.3 us)
Async XLA Ops:
  6.5 104.5 %copy-start.4 = (bf16[128,2048]{1,0:T(8,128)(2,1)S(1)}, bf16[128,2048]{1,0:T(8,128)(2,1)}, u32[]{:S(2)}) copy-start(bf16[128,2048]{1,0:T(8,128)(2,1)} %param.18) | copy-start | bytes 1572868
  6.5 104.5 %copy-start.14 = (f32[2048]{0:T(1024)S(1)}, f32[2048]{0:T(1024)}, u32[]{:S(2)}) copy-start(f32[2048]{0:T(1024)} %param.19) | copy-start | bytes 24580
  6.5 54.8 %all-gather.8.cloned.1.call-start = ((), (), s32[]{:S(2)}) async-start(), calls=%async_computation | async-start | bytes 2359296 | tf_op jit(solution)/shard_map/all_gather | solution.py:93
  7.3 103.8 %all-gather.10.cloned.1.call-start = ((), (), s32[]{:S(2)}) async-start(), calls=%async_computation.1 | async-start | bytes 2359296 | tf_op jit(solution)/shard_map/all_gather | solution.py:91
  8.0 152.9 %all-gather.14.cloned.1.call-start = ((), (), s32[]{:S(2)}) async-start(), calls=%async_computation.3 | async-start | bytes 2359296 | tf_op jit(solution)/shard_map/all_gather | solution.py:90
  8.7 225.5 %all-gather.12.cloned.1.call-start = ((), (), s32[]{:S(2)}) async-start(), calls=%async_computation.2 | async-start | bytes 4718592 | tf_op jit(solution)/shard_map/all_gather | solution.py:92
  9.3 436.7 %all-gather.16.cloned.1.call-start = ((), (), s32[]{:S(2)}) async-start(), calls=%async_computation.4 | async-start | bytes 4718592 | tf_op jit(solution)/shard_map/all_gather | solution.py:94
  9.9 603.4 %all-reduce.3.cloned.1.call-start = ((), (), s32[]{:S(2)}) async-start(), calls=%async_computation.5 | async-start | bytes 1048576 | tf_op jit(solution)/shard_map/psum | solution.py:155
  12.0 152.2 %copy-start.13 = (f32[128,16]{0,1:T(8,128)S(1)}, f32[128,16]{0,1:T(8,128)}, u32[]{:S(2)}) copy-start(f32[128,16]{0,1:T(8,128)} %param.25) | copy-start | bytes 24580
  281.7 8.1 %copy-start.1 = (f32[2,16,64,64]{3,2,1,0:T(8,128)S(1)}, f32[2,16,64,64]{3,2,1,0:T(8,128)}, u32[]{:S(2)}) copy-start(f32[2,16,64,64]{3,2,1,0:T(8,128)} %get-tuple-element.362) | copy-start | bytes 1572868 | tf_op jit(solution)/shard_map/while
  281.7 8.1 %copy-start.8 = (f32[2,16,64,64]{3,2,1,0:T(8,128)S(1)}, f32[2,16,64,64]{3,2,1,0:T(8,128)}, u32[]{:S(2)}) copy-start(f32[2,16,64,64]{3,2,1,0:T(8,128)} %get-tuple-element.350) | copy-start | bytes 1572868 | tf_op jit(solution)/shard_map/while
  281.7 10.1 %copy-start.3 = (f32[2,16,64,32]{2,0,3,1:T(2,128)S(1)}, f32[2,16,64,32]{2,0,3,1:T(2,128)}, u32[]{:S(2)}) copy-start(f32[2,16,64,32]{2,0,3,1:T(2,128)} %copy-done.2) | copy-start | bytes 786436 | tf_op jit(solution)/shard_map/while
  332.5 8.0 %copy-start.1 = (f32[2,16,64,64]{3,2,1,0:T(8,128)S(1)}, f32[2,16,64,64]{3,2,1,0:T(8,128)}, u32[]{:S(2)}) copy-start(f32[2,16,64,64]{3,2,1,0:T(8,128)} %get-tuple-element.362) | copy-start | bytes 1572868 | tf_op jit(solution)/shard_map/while
  332.5 8.0 %copy-start.8 = (f32[2,16,64,64]{3,2,1,0:T(8,128)S(1)}, f32[2,16,64,64]{3,2,1,0:T(8,128)}, u32[]{:S(2)}) copy-start(f32[2,16,64,64]{3,2,1,0:T(8,128)} %get-tuple-element.350) | copy-start | bytes 1572868 | tf_op jit(solution)/shard_map/while
  332.5 10.0 %copy-start.3 = (f32[2,16,64,32]{2,0,3,1:T(2,128)S(1)}, f32[2,16,64,32]{2,0,3,1:T(2,128)}, u32[]{:S(2)}) copy-start(f32[2,16,64,32]{2,0,3,1:T(2,128)} %copy-done.2) | copy-start | bytes 786436 | tf_op jit(solution)/shard_map/while
  342.6 7.1 copy-start
  385.3 7.7 %copy-start.6 = (f32[2,16,64,64]{3,2,1,0:T(8,128)S(1)}, f32[2,16,64,64]{3,2,1,0:T(8,128)}, u32[]{:S(2)}) copy-start(f32[2,16,64,64]{3,2,1,0:T(8,128)} %get-tuple-element.377) | copy-start | bytes 1572868 | tf_op jit(solution)/shard_map/while
  432.5 7.7 %copy-start.6 = (f32[2,16,64,64]{3,2,1,0:T(8,128)S(1)}, f32[2,16,64,64]{3,2,1,0:T(8,128)}, u32[]{:S(2)}) copy-start(f32[2,16,64,64]{3,2,1,0:T(8,128)} %get-tuple-element.377) | copy-start | bytes 1572868 | tf_op jit(solution)/shard_map/while
  443.9 8.2 %copy-start.10 = (bf16[256,1536]{1,0:T(8,128)(2,1)S(1)}, bf16[256,1536]{1,0:T(8,128)(2,1)}, u32[]{:S(2)}) copy-start(bf16[256,1536]{1,0:T(8,128)(2,1)} %param.30) | copy-start | bytes 2359300
  450.5 184.5 %all-gather.18.cloned.1.call-start = ((), (), s32[]{:S(2)}) async-start(), calls=%async_computation.6 | async-start | bytes 7077888 | tf_op jit(solution)/shard_map/all_gather | solution.py:148
  451.3 283.5 %all-gather.20.cloned.1.call-start = ((), (), s32[]{:S(2)}) async-start(), calls=%async_computation.7 | async-start | bytes 7077888 | tf_op jit(solution)/shard_map/all_gather | solution.py:150
  452.0 308.2 %all-reduce.5.cloned.1.call-start = ((), (), s32[]{:S(2)}) async-start(), calls=%async_computation.8 | async-start | bytes 1048576 | tf_op jit(solution)/shard_map/psum | solution.py:164
  452.1 41.7 %collective-permute-start = (bf16[256,1536]{1,0:T(8,128)(2,1)S(1)}, bf16[256,1536]{1,0:T(8,128)(2,1)S(1)}, u32[]{:S(2)}, u32[]{:S(2)}) collective-permute-start(bf16[256,1536]{1,0:T(8,128)(2,1)S(1)} %copy-done.10), channel_id=1, source_target_pairs={{0,2},{2,4},{4,6},{6,8},{8,10},{10,12},{12,14},{14,0},{1,3},{3,5},... | collective-permute-start | bytes 2359304 | tf_op jit(solution)/shard_map/ppermute | solution.py:135
  452.7 45.2 %collective-permute-start.1 = (bf16[256,1536]{1,0:T(8,128)(2,1)S(1)}, bf16[256,1536]{1,0:T(8,128)(2,1)}, u32[]{:S(2)}, u32[]{:S(2)}) collective-permute-start(bf16[256,1536]{1,0:T(8,128)(2,1)S(1)} %copy-done.10), channel_id=1, source_target_pairs={{0,14},{2,0},{4,2},{6,4},{8,6},{10,8},{12,10},{14,12},{1,15},{3,1}... | collective-permute-start | bytes 2359304 | tf_op jit(solution)/shard_map/ppermute | solution.py:141
  493.8 4.7 copy-start.11
  493.8 33.7 %collective-permute-start.2 = (bf16[256,1536]{1,0:T(8,128)(2,1)S(1)}, bf16[256,1536]{1,0:T(8,128)(2,1)}, u32[]{:S(2)}, u32[]{:S(2)}) collective-permute-start(bf16[256,1536]{1,0:T(8,128)(2,1)S(1)} %collective-permute-done), channel_id=1, source_target_pairs={{0,2},{2,4},{4,6},{6,8},{8,10},{10,12},{12,14},{14,0},{1,3},{3,5},... | collective-permute-start | bytes 2359304 | tf_op jit(solution)/shard_map/ppermute | solution.py:135
  497.9 36.9 %collective-permute-start.3 = (bf16[256,1536]{1,0:T(8,128)(2,1)}, bf16[256,1536]{1,0:T(8,128)(2,1)}, u32[]{:S(2)}, u32[]{:S(2)}) collective-permute-start(bf16[256,1536]{1,0:T(8,128)(2,1)} %collective-permute-done.1), channel_id=1, source_target_pairs={{0,14},{2,0},{4,2},{6,4},{8,6},{10,8},{12,10},{14,12},{1,15},{3,1}... | collective-permute-start | bytes 2359304 | tf_op jit(solution)/shard_map/ppermute | solution.py:141
  527.6 53.3 %collective-permute-start.4 = (bf16[256,1536]{1,0:T(8,128)(2,1)}, bf16[256,1536]{1,0:T(8,128)(2,1)S(1)}, u32[]{:S(2)}, u32[]{:S(2)}) collective-permute-start(bf16[256,1536]{1,0:T(8,128)(2,1)} %collective-permute-done.2), channel_id=1, source_target_pairs={{0,2},{2,4},{4,6},{6,8},{8,10},{10,12},{12,14},{14,0},{1,3},{3,5},... | collective-permute-start | bytes 2359304 | tf_op jit(solution)/shard_map/ppermute | solution.py:135
  532.9 80.4 %copy-start.5 = (bf16[128,2048]{1,0:T(8,128)(2,1)S(1)}, bf16[128,2048]{1,0:T(8,128)(2,1)}, u32[]{:S(2)}) copy-start(bf16[128,2048]{1,0:T(8,128)(2,1)} %param.18) | copy-start | bytes 1572868
  533.9 101.2 %copy-start.15 = (f32[2048]{0:T(1024)S(1)}, f32[2048]{0:T(1024)}, u32[]{:S(2)}) copy-start(f32[2048]{0:T(1024)} %param.28) | copy-start | bytes 24580
  534.8 59.8 %collective-permute-start.5 = (bf16[256,1536]{1,0:T(8,128)(2,1)}, bf16[256,1536]{1,0:T(8,128)(2,1)S(1)}, u32[]{:S(2)}, u32[]{:S(2)}) collective-permute-start(bf16[256,1536]{1,0:T(8,128)(2,1)} %collective-permute-done.3), channel_id=1, source_target_pairs={{0,14},{2,0},{4,2},{6,4},{8,6},{10,8},{12,10},{14,12},{1,15},{3,1}... | collective-permute-start | bytes 2359304 | tf_op jit(solution)/shard_map/ppermute | solution.py:141
  580.8 31.5 %collective-permute-start.6 = (bf16[256,1536]{1,0:T(8,128)(2,1)S(1)}, bf16[256,1536]{1,0:T(8,128)(2,1)S(1)}, u32[]{:S(2)}, u32[]{:S(2)}) collective-permute-start(bf16[256,1536]{1,0:T(8,128)(2,1)S(1)} %collective-permute-done.4), channel_id=1, source_target_pairs={{0,2},{2,4},{4,6},{6,8},{8,10},{10,12},{12,14},{14,0},{1,3},{3,5},... | collective-permute-start | bytes 2359304 | tf_op jit(solution)/shard_map/ppermute | solution.py:135
  (8 other events, 15.8 us)
Sparse Core Ops, SparseCore 0:
  9.5 51.7 all-gather.7
  63.4 47.6 all-gather.9
  113.2 47.6 all-gather.13
  162.8 71.3 all-gather.11
  236.2 71.3 all-gather.15
  450.7 17.1 all-reduce.2
  470.0 164.9 all-gather.17
  637.2 97.4 all-gather.19
  743.4 16.7 all-reduce.4
